TPU v7x, 32 devices: a whole 2x2x4 slice. The times are simulated.
32 devices in a mesh: dp: 4 (over y, x), kv: 4 (over z), tp: 2 (over core).
Axes of the slice: x: 2, y: 2, z: 4, core: 2. Of those that a mesh axis runs over, the one named last changes fastest.
Arguments:
- hidden: bfloat16 [2048, 16], P(('kv', 'tp'), 'dp'), parts along dimension 1, may hold values from -20 to 20
- mixer_gain: float32 [2048], replicated, may hold values from 0.1 to 1.9
- gate_proj: bfloat16 [2048, 64, 64], P(None, 'kv', 'tp'), may hold values from -0.125 to 0.125
- inner_proj: bfloat16 [2048, 64, 64], P(None, 'kv', 'tp'), may hold values from -0.125 to 0.125
- input_proj: bfloat16 [2048, 1024], P(None, 'kv'), may hold values from -0.125 to 0.125
- output_proj: bfloat16 [2048, 1024], P(None, 'kv'), may hold values from -0.125 to 0.125
- step_proj: bfloat16 [2048, 64], replicated, may hold values from -0.125 to 0.125
- step_bias: float32 [64], replicated, may hold values from -3 to -0.5
- decay_log: float32 [64], replicated, may hold values from -3 to 1
- skip_gain: float32 [64], replicated, may hold values from 0.3 to 1.5
- taps_inner: float32 [4, 64, 64], P(None, None, 'tp'), may hold values from -3 to 3
- taps_input: float32 [4, 1024], replicated, may hold values from -3 to 3
- taps_output: float32 [4, 1024], replicated, may hold values from -3 to 3
- recent_inner: bfloat16 [16, 3, 64, 64], P(('dp', 'kv'), None, None, 'tp'), parts along dimension 0, may hold values from -6 to 6
- recent_input: bfloat16 [16, 3, 1024], P(('dp', 'kv')), parts along dimension 0, may hold values from -6 to 6
- recent_output: bfloat16 [16, 3, 1024], P(('dp', 'kv')), parts along dimension 0, may hold values from -6 to 6
- states: float32 [16, 64, 64, 128], P(('dp', 'kv'), None, 'tp'), parts along dimension 0, may hold values from -4 to 4
- block_inner: bfloat16 [16, 128, 64, 64], P(('dp', 'kv'), None, None, 'tp'), parts along dimension 0, may hold values from -6 to 6
- block_input: bfloat16 [16, 128, 1024], P(('dp', 'kv')), parts along dimension 0, may hold values from -4 to 4
- block_decay: float32 [16, 128, 64], P(('dp', 'kv')), parts along dimension 0
- lengths: int32 [16], P(('dp', 'kv')), parts along dimension 0, may hold values from 1 to 128, 170 in all
- norm_gain: float32 [64, 64], P(None, 'tp'), may hold values from 0.1 to 1.9
- mixer_out: bfloat16 [64, 64, 2048], P('kv', 'tp'), may hold values from -0.125 to 0.125
- channel_gain: float32 [2048], replicated, may hold values from 0.1 to 1.9
- expand_gate: bfloat16 [2048, 5632], P(None, ('kv', 'tp')), may hold values from -0.125 to 0.125
- expand_value: bfloat16 [2048, 5632], P(None, ('kv', 'tp')), may hold values from -0.125 to 0.125
- reduce_proj: bfloat16 [5632, 2048], P(('kv', 'tp')), may hold values from -0.109375 to 0.109375
Outputs:
- layer_out: bfloat16 [2048, 16], P(('kv', 'tp'), 'dp'), parts along dimension 1
There are 4 independent parts, one for each index of `dp`. A program takes and returns all parts, laid end to end along the dimension named above; an argument that names none is the same for every part. Nothing has to cross between parts.
All inputs are finite; a program needn't handle non-finite values. No bound on the sum of `lengths` on one device may be relied on, other than what follows from the above.
Results may differ from a plain program's by a relative error of at most 0.01.
Values may be sent and summed in bfloat16 or wider, within the bound.
No kernel may reach another device: no remote copies, remote signals or barrier semaphores. Data moves between devices by JAX's collectives and lax.ppermute only.
A program may use at most 64 MiB of HBM per device.

v0:
```python
import jax
import jax.numpy as jnp
from jax import lax
from jax.sharding import PartitionSpec as P

MIXER_HEADS = 64
HEAD_DIM = 64
GROUPS = 8
STATE = 128
OPEN_BLOCK_SPAN = 128
epsilon = 1e-05


def short_conv(recent, newest, taps):
    window = jnp.concatenate(
        [recent.astype(jnp.float32), newest.astype(jnp.float32)[:, None]], axis=1
    )
    return jax.nn.silu(jnp.sum(window * taps[None], axis=1))


def shards(
    hidden,
    mixer_gain,
    gate_proj,
    inner_proj,
    input_proj,
    output_proj,
    step_proj,
    step_bias,
    decay_log,
    skip_gain,
    taps_inner,
    taps_input,
    taps_output,
    recent_inner,
    recent_input,
    recent_output,
    states,
    block_inner,
    block_input,
    block_decay,
    lengths,
    norm_gain,
    mixer_out,
    channel_gain,
    expand_gate,
    expand_value,
    reduce_proj,
):
    rows_own = hidden.shape[0]
    seq_all = hidden.shape[1]
    seq_dev = states.shape[0]
    half_dim = states.shape[2]
    width = rows_own * lax.axis_size("kv") * lax.axis_size("tp")
    offset = (lax.axis_index("kv") * lax.axis_size("tp") + lax.axis_index("tp")) * rows_own
    own_start = lax.axis_index("kv") * seq_dev
    whole_rows = lax.all_gather(hidden, ("kv", "tp"), axis=0, tiled=True)
    whole_f = whole_rows.astype(jnp.float32)
    rms_in = lax.rsqrt(jnp.mean(whole_f * whole_f, axis=0) + epsilon)
    normed_in = (whole_f * mixer_gain[:, None]).astype(jnp.bfloat16)
    gate_part = (
        rms_in[:, None, None]
        * jnp.einsum("ds,dhp->shp", normed_in, gate_proj, preferred_element_type=jnp.float32)
    ).astype(jnp.bfloat16)
    inner_part = (
        rms_in[:, None, None]
        * jnp.einsum("ds,dhp->shp", normed_in, inner_proj, preferred_element_type=jnp.float32)
    ).astype(jnp.bfloat16)
    input_part = (
        rms_in[:, None]
        * jnp.einsum("ds,dk->sk", normed_in, input_proj, preferred_element_type=jnp.float32)
    ).astype(jnp.bfloat16)
    output_part = (
        rms_in[:, None]
        * jnp.einsum("ds,dk->sk", normed_in, output_proj, preferred_element_type=jnp.float32)
    ).astype(jnp.bfloat16)
    own_cols = lax.dynamic_slice_in_dim(normed_in, own_start, seq_dev, 1)
    own_rms = lax.dynamic_slice_in_dim(rms_in, own_start, seq_dev, 0)
    step_pre = (
        own_rms[:, None]
        * jnp.einsum("ds,dh->sh", own_cols, step_proj, preferred_element_type=jnp.float32)
    ).astype(jnp.bfloat16)
    gate_pre, inner_pre, input_pre, output_pre = (
        lax.all_to_all(gate_part, "kv", split_axis=0, concat_axis=1, tiled=True),
        lax.all_to_all(inner_part, "kv", split_axis=0, concat_axis=1, tiled=True),
        lax.all_to_all(input_part, "kv", split_axis=0, concat_axis=1, tiled=True),
        lax.all_to_all(output_part, "kv", split_axis=0, concat_axis=1, tiled=True),
    )
    conv_inner = short_conv(recent_inner, inner_pre, taps_inner)
    conv_input = short_conv(recent_input, input_pre, taps_input)
    conv_output = short_conv(recent_output, output_pre, taps_output).astype(jnp.bfloat16)
    step = jax.nn.softplus(step_pre.astype(jnp.float32) + step_bias[None, :])
    new_decay = -jnp.exp(decay_log)[None, :] * step
    per_group = MIXER_HEADS // GROUPS
    live = (jnp.arange(OPEN_BLOCK_SPAN, dtype=jnp.int32)[None, :] < lengths[:, None]).astype(
        jnp.float32
    )
    masked = block_decay * live[:, :, None]
    cached = jnp.sum(masked, axis=1)
    tail = new_decay[:, None, :] + cached[:, None, :] - jnp.cumsum(masked, axis=1)
    total = new_decay + cached
    readout = conv_output.reshape(seq_dev, GROUPS, STATE)
    score = jnp.einsum(
        "sgn,sjgn->sgj",
        readout,
        block_input.reshape(seq_dev, OPEN_BLOCK_SPAN, GROUPS, STATE),
        preferred_element_type=jnp.float32,
    )
    score_heads = jnp.repeat(score, per_group, axis=1)
    weight = (live[:, None, :] * jnp.exp(jnp.swapaxes(tail, 1, 2)) * score_heads).astype(
        jnp.bfloat16
    )
    from_block = jnp.einsum(
        "shj,sjhp->shp", weight, block_inner, preferred_element_type=jnp.float32
    )
    readout_f = readout.astype(jnp.float32)
    grouped = states.reshape(seq_dev, GROUPS, per_group, half_dim, STATE)
    from_state = jnp.einsum(
        "sgn,sgrpn->sgrp", readout_f, grouped, precision=lax.Precision.HIGHEST
    ).reshape(seq_dev, MIXER_HEADS, half_dim)
    own_score = jnp.repeat(
        jnp.sum(readout_f * conv_input.reshape(seq_dev, GROUPS, STATE), axis=-1), per_group, axis=1
    )
    mix = (
        from_block
        + jnp.exp(total)[:, :, None] * from_state
        + (own_score * step)[:, :, None] * conv_inner
        + skip_gain[None, :, None] * conv_inner
    )
    gated_raw = mix * jax.nn.silu(gate_pre.astype(jnp.float32))
    part_squares = jnp.sum(gated_raw * gated_raw, axis=(1, 2))
    gated = (gated_raw * norm_gain[None]).astype(jnp.bfloat16)
    placed = lax.dynamic_update_slice_in_dim(
        jnp.zeros((seq_all,), jnp.float32), part_squares, own_start, 0
    )
    gate_squares = lax.psum(placed, ("kv", "tp"))
    rms_gate = lax.rsqrt(gate_squares / (MIXER_HEADS * HEAD_DIM) + epsilon)
    by_head = lax.all_to_all(gated, "kv", split_axis=1, concat_axis=0, tiled=True)
    columns = mixer_out
    mixed_full = rms_gate[None, :] * lax.psum(
        jnp.einsum("hpd,shp->ds", columns, by_head, preferred_element_type=jnp.float32),
        ("kv", "tp"),
    )
    mid_full = (whole_f + mixed_full).astype(jnp.bfloat16)
    mid = lax.dynamic_slice_in_dim(mid_full, offset, rows_own, 0)
    full_f = mid_full.astype(jnp.float32)
    mid_squares = jnp.sum(full_f * full_f, axis=0)
    normed_full = (full_f * channel_gain[:, None]).astype(jnp.bfloat16)
    gate_sum = jnp.einsum("ds,df->sf", normed_full, expand_gate, preferred_element_type=jnp.float32)
    value_sum = jnp.einsum(
        "ds,df->sf", normed_full, expand_value, preferred_element_type=jnp.float32
    )
    rms_mid = lax.rsqrt(mid_squares / width + epsilon)
    act = (jax.nn.silu(rms_mid[:, None] * gate_sum) * (rms_mid[:, None] * value_sum)).astype(
        jnp.bfloat16
    )
    columns = reduce_proj
    channel = lax.psum_scatter(
        jnp.einsum("fd,sf->ds", columns, act, preferred_element_type=jnp.float32),
        ("kv", "tp"),
        scatter_dimension=0,
        tiled=True,
    )
    return (mid.astype(jnp.float32) + channel).astype(jnp.bfloat16)


def solution(mesh):
    return jax.shard_map(
        shards,
        mesh=mesh,
        in_specs=(
            P(("kv", "tp"), "dp"),
            P(),
            P(None, "kv", "tp"),
            P(None, "kv", "tp"),
            P(None, "kv"),
            P(None, "kv"),
            P(),
            P(),
            P(),
            P(),
            P(None, None, "tp"),
            P(),
            P(),
            P(("dp", "kv"), None, None, "tp"),
            P(("dp", "kv"), None, None),
            P(("dp", "kv"), None, None),
            P(("dp", "kv"), None, "tp", None),
            P(("dp", "kv"), None, None, "tp"),
            P(("dp", "kv"), None, None),
            P(("dp", "kv"), None, None),
            P(("dp", "kv")),
            P(None, "tp"),
            P("kv", "tp", None),
            P(),
            P(None, ("kv", "tp")),
            P(None, ("kv", "tp")),
            P(("kv", "tp"), None),
        ),
        out_specs=P(("kv", "tp"), "dp"),
        check_vma=False,
    )
```

profile of v0, /device:TPU:0, one launch (start us, length us, event | category | flops | bytes accessed | tf_op | source)
XLA Modules:
  0.0 156.3 jit_solution(15144254045306652727)
XLA Ops:
  6.5 14.7 %all_gather.3 = bf16[2048,4]{0,1:T(4,128)(2,1)S(1)} all-gather(bf16[256,4]{0,1:T(4,128)(2,1)} %param.27), channel_id=1, replica_groups=mesh['dp'=4,'kv'=4,'tp'=2] {'kv','tp'}, dimensions={0}, use_global_device_ids=true | all-gather | bytes 18432 | tf_op jit(solution)/shard_map/all_gather | solution.py:57
  21.3 0.8 fusion.15
  22.1 1.4 fusion.7
  23.5 0.0 copy-start.2
  23.6 0.5 broadcast.167
  24.1 0.6 reduce.13
  24.8 0.6 reshape.385
  25.4 3.4 %all-to-all-start = ((bf16[4,2,128]{2,1,0:T(2,128)(2,1)}), bf16[4,2,128]{2,1,0:T(2,128)(2,1)S(1)}, u32[]{:S(2)}, u32[]{:S(2)}) async-start(bf16[4,2,128]{2,1,0:T(2,128)(2,1)} %reshape.385), calls=%async_computation | async-start | bytes 4096 | tf_op jit(solution)/shard_map/all_to_all | solution.py:87
  29.5 1.4 fusion.6
  31.0 3.1 %fusion.1 = bf16[4,16,32]{2,0,1:T(4,128)(2,1)S(1)} fusion(bf16[2048,16,32]{0,2,1:T(8,128)(2,1)} %param.29, bf16[2048,4]{0,1:T(4,128)(2,1)S(1)} %get-tuple-element.16, f32[4]{0:T(128)S(1)} %add_rsqrt_fusion.2), kind=kOutput, calls=%fused_computation.5 | convolution fusion | flops 8392704 | bytes 2117648 | tf_op jit(solution)/shard_map/ds,dhp->shp/dot_general | solution.py:63
  34.1 0.0 copy-start.6
  34.1 1.5 fusion
  35.6 0.0 copy-start.8
  35.6 0.6 reduce.12
  36.2 0.6 reshape.387
  36.8 0.1 copy.48
  36.9 5.1 %all-to-all-start.1 = ((bf16[4,2,128]{2,1,0:T(2,128)(2,1)}), bf16[4,2,128]{2,1,0:T(2,128)(2,1)S(1)}, u32[]{:S(2)}, u32[]{:S(2)}) async-start(bf16[4,2,128]{2,1,0:T(2,128)(2,1)} %reshape.387), calls=%async_computation.1 | async-start | bytes 4096 | tf_op jit(solution)/shard_map/all_to_all | solution.py:86
  42.0 0.6 fusion.58
  42.7 0.6 dynamic_slice.9
  43.3 0.7 reshape.381
  44.0 0.7 reshape.383
  44.6 0.2 copy.70
  44.8 0.2 reduce_window_sum.11
  45.0 2.5 %all-to-all-done.1 = bf16[4,2,128]{2,1,0:T(2,128)(2,1)S(1)} async-done(((bf16[4,2,128]{2,1,0:T(2,128)(2,1)}), bf16[4,2,128]{2,1,0:T(2,128)(2,1)S(1)}, u32[]{:S(2)}, u32[]{:S(2)}) %all-to-all-start.1) | async-done | bytes 2080 | tf_op jit(solution)/shard_map/all_to_all | solution.py:86
  47.5 3.2 %all-to-all-start.2 = ((bf16[4,2,256]{2,1,0:T(2,128)(2,1)}), bf16[4,2,256]{2,1,0:T(2,128)(2,1)S(1)}, u32[]{:S(2)}, u32[]{:S(2)}) async-start(bf16[4,2,256]{2,1,0:T(2,128)(2,1)} %reshape.383), calls=%async_computation.2 | async-start | bytes 8192 | tf_op jit(solution)/shard_map/all_to_all | solution.py:85
  50.8 0.8 multiply_reduce_fusion.3
  51.6 0.1 fusion.49
  51.7 0.1 broadcast_in_dim.10
  51.8 0.1 broadcast_in_dim.11
  51.9 0.2 fusion.45
  52.1 0.1 copy.50
  52.2 3.4 %fusion.43 = f32[8,1,8,32]{3,1,2,0:T(1,128)S(1)} fusion(f32[8,8,32,128]{3,2,1,0:T(8,128)} %bitcast.136, bf16[8,128,1,1]{1,0,2,3:T(8,128)(2,1)S(1)} %get-tuple-element.17), kind=kOutput, calls=%fused_computation.72 | convolution fusion | flops 3145728 | bytes 1058816 | tf_op jit(solution)/shard_map/sgn,sgrpn->sgrp/dot_general | solution.py:118
  55.6 1.8 %fusion.57 = (f32[64]{0:T(128)S(1)}, f32[64]{0:T(128)S(1)}, f32[64]{0:T(128)S(1)}) fusion(f32[64]{0:T(128)} %get-tuple-element.13, f32[64]{0:T(128)} %param.35, f32[64]{0:T(128)S(1)} %broadcast_in_dim.11, f32[64]{0:T(128)} %param.34, bf16[2048,64]{0,1:T(8,128)(2,1)} %param.33, bf16[2048,4]{0,1:T(4,128)(2,1)S(1)} %get-tuple-element.16, s32[]{:T(128)S(6)} %select_n.13, ...), kind=kOutput, calls=%fused_computation.90 | convolution fusion | flops 263040 | bytes 272392 | tf_op jit(solution)/shard_map/ds,dh->sh/dot_general | solution.py:81
  57.4 0.8 fusion.19
  58.1 0.1 copy.74
  58.2 0.0 all-to-all-done.2
  58.2 5.1 %all-to-all-start.3 = ((bf16[4,2,256]{2,1,0:T(2,128)(2,1)}), bf16[4,2,256]{2,1,0:T(2,128)(2,1)S(1)}, u32[]{:S(2)}, u32[]{:S(2)}) async-start(bf16[4,2,256]{2,1,0:T(2,128)(2,1)} %reshape.381), calls=%async_computation.3 | async-start | bytes 8192 | tf_op jit(solution)/shard_map/all_to_all | solution.py:84
  63.3 1.4 multiply_reduce_fusion
  64.7 0.1 copy.51
  64.7 0.1 copy.67
  64.8 0.1 reshape.384
  64.9 0.1 copy.54
  65.0 3.9 %all-to-all-done.3 = bf16[4,2,256]{2,1,0:T(2,128)(2,1)S(1)} async-done(((bf16[4,2,256]{2,1,0:T(2,128)(2,1)}), bf16[4,2,256]{2,1,0:T(2,128)(2,1)S(1)}, u32[]{:S(2)}, u32[]{:S(2)}) %all-to-all-start.3) | async-done | bytes 4128 | tf_op jit(solution)/shard_map/all_to_all | solution.py:84
  68.8 0.1 reshape.382
  68.9 0.1 copy.57
  69.0 1.3 multiply_reduce_fusion.2
  70.3 0.1 copy.58
  70.5 0.7 reduce.14
  71.2 0.7 reshape.389
  71.9 3.2 %all-to-all-start.4 = ((bf16[4,2,256]{2,1,0:T(2,128)(2,1)}), bf16[4,2,256]{2,1,0:T(2,128)(2,1)S(1)}, u32[]{:S(2)}, u32[]{:S(2)}) async-start(bf16[4,2,256]{2,1,0:T(2,128)(2,1)} %reshape.389), calls=%async_computation.4 | async-start | bytes 8192 | tf_op jit(solution)/shard_map/all_to_all | solution.py:138
  75.1 0.0 reduce-scatter.4.cloned.1.call-start
  75.2 0.8 dynamic_update_slice.3
  75.9 4.7 %all-to-all-done.4 = bf16[4,2,256]{2,1,0:T(2,128)(2,1)S(1)} async-done(((bf16[4,2,256]{2,1,0:T(2,128)(2,1)}), bf16[4,2,256]{2,1,0:T(2,128)(2,1)S(1)}, u32[]{:S(2)}, u32[]{:S(2)}) %all-to-all-start.4) | async-done | bytes 4128 | tf_op jit(solution)/shard_map/all_to_all | solution.py:138
  80.7 0.1 reshape.390
  80.8 2.0 %convolution_bitcast_fusion.1 = f32[2048,4]{0,1:T(4,128)S(1)} fusion(bf16[16,32,2048]{2,1,0:T(8,128)(2,1)} %param.49, bf16[4,16,32]{2,1,0:T(8,128)(2,1)S(1)} %bitcast.141), kind=kOutput, calls=%fused_computation.1 | convolution fusion | flops 8388608 | bytes 2134016 | tf_op jit(solution)/shard_map/hpd,shp->ds/dot_general | solution.py:141
  82.8 26.3 %all-reduce = (f32[2048,4]{0,1:T(4,128)S(1)}, f32[4]{0:T(128)S(1)}) all-reduce(f32[2048,4]{0,1:T(4,128)S(1)} %convolution_bitcast_fusion.1, f32[4]{0:T(128)S(1)} %dynamic_update_slice.3), channel_id=1, replica_groups=mesh['dp'=4,'kv'=4,'tp'=2] {'kv','tp'}, use_global_device_ids=true, to_apply=%region_9.10 | all-reduce | flops 8196 | bytes 65568 | tf_op jit(solution)/shard_map/psum | solution.py:140
  109.1 0.2 fusion.13
  109.3 2.7 %convolution_multiply_fusion.3 = f32[4,704]{1,0:T(4,128)S(1)} fusion(bf16[2048,704]{0,1:T(8,128)(2,1)} %param.51, bf16[2048,4]{0,1:T(4,128)(2,1)S(1)} %get-tuple-element.8, f32[2048]{0:T(1024)S(1)} %copy-done.4, f32[4]{0:T(128)S(1)} %add_rsqrt_fusion), kind=kOutput, calls=%fused_computation.8 | convolution fusion | flops 11561728 | bytes 2919440 | tf_op jit(solution)/shard_map/ds,df->sf/dot_general | solution.py:149
  112.0 3.5 %convolution_bitcast_fusion = f32[2048,4]{0,1:T(4,128)S(1)} fusion(bf16[704,2048]{1,0:T(8,128)(2,1)S(1)} %copy-done, bf16[2048,704]{0,1:T(8,128)(2,1)} %param.52, f32[4,704]{1,0:T(4,128)S(1)} %convolution_multiply_fusion.3, bf16[2048,4]{0,1:T(4,128)(2,1)S(1)} %get-tuple-element.8, f32[2048]{0:T(1024)S(1)} %copy-done.4, f32[4]{0:T(128)S(1)} %add_rsqrt_fusion), kind=kOutput, calls=%fused_computation | convolution fusion | flops 23112960 | bytes 5835792 | tf_op jit(solution)/shard_map/fd,sf->ds/dot_general | solution.py:159
  115.5 1.4 copy.71
  116.8 0.0 reduce-scatter.4.cloned.1.call-update
  116.9 31.0 %reduce-scatter.4.cloned.1.call-done = f32[256,4]{1,0:T(8,128)} async-done(((f32[2048,4]{1,0:T(8,128)}), f32[256,4]{1,0:T(8,128)}) %reduce-scatter.4.cloned.1.call-update) | async-done | bytes 4112
  147.8 1.0 copy.72
  148.8 0.6 add_convert_fusion
  (31 shorter events, 0.2 us)
Async XLA Ops:
  6.5 105.4 %copy-start = (bf16[704,2048]{1,0:T(8,128)(2,1)S(1)}, bf16[704,2048]{1,0:T(8,128)(2,1)}, u32[]{:S(2)}) copy-start(bf16[704,2048]{1,0:T(8,128)(2,1)} %param.53) | copy-start | bytes 8650756
  23.5 13.3 %copy-start.5 = (f32[1,128,64]{1,2,0:T(8,128)S(1)}, f32[1,128,64]{1,2,0:T(8,128)}, u32[]{:S(2)}) copy-start(f32[1,128,64]{1,2,0:T(8,128)} %param.46) | copy-start | bytes 98308
  23.5 21.1 %copy-start.2 = (bf16[1,128,1024]{2,1,0:T(8,128)(2,1)S(1)}, bf16[1,128,1024]{2,1,0:T(8,128)(2,1)}, u32[]{:S(2)}) copy-start(bf16[1,128,1024]{2,1,0:T(8,128)(2,1)} %param.45) | copy-start | bytes 786436
  25.4 11.5 %all-to-all-start = ((bf16[4,2,128]{2,1,0:T(2,128)(2,1)}), bf16[4,2,128]{2,1,0:T(2,128)(2,1)S(1)}, u32[]{:S(2)}, u32[]{:S(2)}) async-start(bf16[4,2,128]{2,1,0:T(2,128)(2,1)} %reshape.385), calls=%async_computation | async-start | bytes 4096 | tf_op jit(solution)/shard_map/all_to_all | solution.py:87
  28.7 5.3 %copy-start.1 = (bf16[2048,16,32]{0,2,1:T(8,128)(2,1)S(1)}, bf16[2048,16,32]{0,2,1:T(8,128)(2,1)}, u32[]{:S(2)}) copy-start(bf16[2048,16,32]{0,2,1:T(8,128)(2,1)} %param.30) | copy-start | bytes 6291460
  34.1 34.9 %copy-start.6 = (bf16[1,3,64,32]{2,3,1,0:T(8,128)(2,1)S(1)}, bf16[1,3,64,32]{2,3,1,0:T(8,128)(2,1)}, u32[]{:S(2)}) copy-start(bf16[1,3,64,32]{2,3,1,0:T(8,128)(2,1)} %param.40) | copy-start | bytes 36868
  34.1 36.2 %copy-start.7 = (f32[64,32]{0,1:T(8,128)S(1)}, f32[64,32]{0,1:T(8,128)}, u32[]{:S(2)}) copy-start(f32[64,32]{0,1:T(8,128)} %param.48) | copy-start | bytes 24580
  35.6 8.4 %copy-start.8 = (f32[128]{0:T(128)}, f32[128]{0:T(128)S(1)}, u32[]{:S(2)}) copy-start(f32[128]{0:T(128)S(1)} %compare_convert_fusion) | copy-start | bytes 1540
  36.9 10.6 %all-to-all-start.1 = ((bf16[4,2,128]{2,1,0:T(2,128)(2,1)}), bf16[4,2,128]{2,1,0:T(2,128)(2,1)S(1)}, u32[]{:S(2)}, u32[]{:S(2)}) async-start(bf16[4,2,128]{2,1,0:T(2,128)(2,1)} %reshape.387), calls=%async_computation.1 | async-start | bytes 4096 | tf_op jit(solution)/shard_map/all_to_all | solution.py:86
  44.8 24.2 %copy-start.3 = (f32[4,64,32]{1,2,0:T(8,128)S(1)}, f32[4,64,32]{1,2,0:T(8,128)}, u32[]{:S(2)}) copy-start(f32[4,64,32]{1,2,0:T(8,128)} %param.37) | copy-start | bytes 98308
  47.5 10.7 %all-to-all-start.2 = ((bf16[4,2,256]{2,1,0:T(2,128)(2,1)}), bf16[4,2,256]{2,1,0:T(2,128)(2,1)S(1)}, u32[]{:S(2)}, u32[]{:S(2)}) async-start(bf16[4,2,256]{2,1,0:T(2,128)(2,1)} %reshape.383), calls=%async_computation.2 | async-start | bytes 8192 | tf_op jit(solution)/shard_map/all_to_all | solution.py:85
  50.8 58.5 %copy-start.4 = (f32[2048]{0:T(1024)S(1)}, f32[2048]{0:T(1024)}, u32[]{:S(2)}) copy-start(f32[2048]{0:T(1024)} %param.50) | copy-start | bytes 24580
  58.2 10.6 %all-to-all-start.3 = ((bf16[4,2,256]{2,1,0:T(2,128)(2,1)}), bf16[4,2,256]{2,1,0:T(2,128)(2,1)S(1)}, u32[]{:S(2)}, u32[]{:S(2)}) async-start(bf16[4,2,256]{2,1,0:T(2,128)(2,1)} %reshape.381), calls=%async_computation.3 | async-start | bytes 8192 | tf_op jit(solution)/shard_map/all_to_all | solution.py:84
  71.9 8.8 %all-to-all-start.4 = ((bf16[4,2,256]{2,1,0:T(2,128)(2,1)}), bf16[4,2,256]{2,1,0:T(2,128)(2,1)S(1)}, u32[]{:S(2)}, u32[]{:S(2)}) async-start(bf16[4,2,256]{2,1,0:T(2,128)(2,1)} %reshape.389), calls=%async_computation.4 | async-start | bytes 8192 | tf_op jit(solution)/shard_map/all_to_all | solution.py:138
  75.1 72.7 %reduce-scatter.4.cloned.1.call-start = ((), (), s32[]{:S(2)}) async-start(), calls=%async_computation.6 | async-start | bytes 1179648
Sparse Core Ops, SparseCore 0:
  117.0 30.8 reduce-scatter.3
where the time goes:
time: 157 us; the launch traced here: 156 us
  waiting for transfers between devices  42.1 us (27%)
  blocking collectives  41 us (26%)
  matrix products  20.9 us (13%)
  starting transfers between devices  20 us (13%)
  between operations  14.4 us (9%)
  other arithmetic  8.9 us (6%)
  local copies, waits for them, and re-layouts  8.85 us (6%)
    unnamed x2, waiting for transfers between devices  31 us
    psum x1, blocking collectives, shards(): lax.psum(jnp.einsum('hpd,shp->ds', columns, by_head, preferred_element_ty...  26.3 us
    all_gather x1, blocking collectives, shards(): whole_rows = lax.all_gather(hidden, ('kv', 'tp'), axis=0, tiled=True)  14.7 us
    unnamed x33, local copies, waits for them, and re-layouts  6.14 us
    all_to_all x1, starting transfers between devices, shards(): lax.all_to_all(input_part, 'kv', split_axis=0, concat_axis=1, tiled=True)  5.1 us
    all_to_all x1, starting transfers between devices, shards(): lax.all_to_all(gate_part, 'kv', split_axis=0, concat_axis=1, tiled=True)  5.06 us
    all_to_all x1, waiting for transfers between devices, shards(): lax.all_to_all(gated, 'kv', split_axis=1, concat_axis=0, tiled=True)  4.73 us
    all_to_all x1, waiting for transfers between devices, shards(): lax.all_to_all(gate_part, 'kv', split_axis=0, concat_axis=1, tiled=True)  3.87 us
  transfers between devices with their start and end apart: 6, of which 4 were waited for; matrix products, arithmetic and copies ran while one was open for 13% of the time, Pallas kernels for 0%

commit v1 on v0

--- a/solution.py
+++ b/solution.py
@@ -9,6 +9,11 @@
 STATE = 128
 OPEN_BLOCK_SPAN = 128
 epsilon = 1e-05
+
+
+def derive_the_teams(inp, mesh_name, row_axis="kv"):
+    all_values = jax.lax.psum(inp, mesh_name)
+    return jax.lax.psum(all_values, row_axis)
 
 
 def short_conv(recent, newest, taps):
@@ -137,9 +142,8 @@
     rms_gate = lax.rsqrt(gate_squares / (MIXER_HEADS * HEAD_DIM) + epsilon)
     by_head = lax.all_to_all(gated, "kv", split_axis=1, concat_axis=0, tiled=True)
     columns = mixer_out
-    mixed_full = rms_gate[None, :] * lax.psum(
-        jnp.einsum("hpd,shp->ds", columns, by_head, preferred_element_type=jnp.float32),
-        ("kv", "tp"),
+    mixed_full = rms_gate[None, :] * derive_the_teams(
+        jnp.einsum("hpd,shp->ds", columns, by_head, preferred_element_type=jnp.float32), "tp"
     )
     mid_full = (whole_f + mixed_full).astype(jnp.bfloat16)
     mid = lax.dynamic_slice_in_dim(mid_full, offset, rows_own, 0)

time: 157 us -> 166 us (1.057)
  blocking collectives: 41 us -> 48 us
    psum x1 -> x3, blocking collectives: 26.3 us -> 33.3 us  [the longest x1 16.2 us: derive_the_teams(): return jax.lax.psum(all_values, row_axis)]
  transfers between devices with their start and end apart: 6 -> 6, of which waited for: 4 -> 4; matrix products, arithmetic and copies ran while one was open for 13% -> 12% of each run, Pallas kernels for 0% -> 0%
where the time goes in v1:
time: 166 us; the launch traced here: 165 us
  blocking collectives  48 us (29%)
  waiting for transfers between devices  43.7 us (26%)
  matrix products  20.9 us (13%)
  starting transfers between devices  20 us (12%)
  between operations  14.4 us (9%)
  other arithmetic  8.89 us (5%)
  local copies, waits for them, and re-layouts  8.84 us (5%)
    unnamed x2, waiting for transfers between devices  31.8 us
    psum x1, blocking collectives, derive_the_teams(): return jax.lax.psum(all_values, row_axis)  16.2 us
    all_gather x1, blocking collectives, shards(): whole_rows = lax.all_gather(hidden, ('kv', 'tp'), axis=0, tiled=True)  14.7 us
    psum x1, blocking collectives, shards(): gate_squares = lax.psum(placed, ('kv', 'tp'))  13.6 us
    unnamed x33, local copies, waits for them, and re-layouts  6.14 us
    all_to_all x1, waiting for transfers between devices, shards(): lax.all_to_all(gated, 'kv', split_axis=1, concat_axis=0, tiled=True)  5.48 us
    all_to_all x1, starting transfers between devices, shards(): lax.all_to_all(input_part, 'kv', split_axis=0, concat_axis=1, tiled=True)  5.1 us
    all_to_all x1, starting transfers between devices, shards(): lax.all_to_all(gate_part, 'kv', split_axis=0, concat_axis=1, tiled=True)  5.06 us
  transfers between devices with their start and end apart: 6, of which 4 were waited for; matrix products, arithmetic and copies ran while one was open for 12% of the time, Pallas kernels for 0%

profile of v1, /device:TPU:0, one launch (start us, length us, event | category | flops | bytes accessed | tf_op | source)
XLA Modules:
  0.0 164.8 jit_solution(403082110130672706)
XLA Ops:
  6.5 14.7 %all_gather.3 = bf16[2048,4]{0,1:T(4,128)(2,1)S(1)} all-gather(bf16[256,4]{0,1:T(4,128)(2,1)} %param.27), channel_id=1, replica_groups=mesh['dp'=4,'kv'=4,'tp'=2] {'kv','tp'}, dimensions={0}, use_global_device_ids=true | all-gather | bytes 18432 | tf_op jit(solution)/shard_map/all_gather | solution.py:62
  21.3 0.8 fusion.15
  22.1 1.4 fusion.7
  23.5 0.0 copy-start.2
  23.6 0.5 broadcast.167
  24.1 0.6 reduce.13
  24.8 0.6 reshape.385
  25.4 3.4 %all-to-all-start = ((bf16[4,2,128]{2,1,0:T(2,128)(2,1)}), bf16[4,2,128]{2,1,0:T(2,128)(2,1)S(1)}, u32[]{:S(2)}, u32[]{:S(2)}) async-start(bf16[4,2,128]{2,1,0:T(2,128)(2,1)} %reshape.385), calls=%async_computation | async-start | bytes 4096 | tf_op jit(solution)/shard_map/all_to_all | solution.py:92
  29.5 1.4 fusion.6
  31.0 3.1 %fusion.1 = bf16[4,16,32]{2,0,1:T(4,128)(2,1)S(1)} fusion(bf16[2048,16,32]{0,2,1:T(8,128)(2,1)} %param.29, bf16[2048,4]{0,1:T(4,128)(2,1)S(1)} %get-tuple-element.14, f32[4]{0:T(128)S(1)} %add_rsqrt_fusion.2), kind=kOutput, calls=%fused_computation.5 | convolution fusion | flops 8392704 | bytes 2117648 | tf_op jit(solution)/shard_map/ds,dhp->shp/dot_general | solution.py:68
  34.1 1.5 fusion
  35.6 0.6 reduce.12
  36.2 0.6 reshape.387
  36.8 0.1 copy.48
  36.9 5.1 %all-to-all-start.1 = ((bf16[4,2,128]{2,1,0:T(2,128)(2,1)}), bf16[4,2,128]{2,1,0:T(2,128)(2,1)S(1)}, u32[]{:S(2)}, u32[]{:S(2)}) async-start(bf16[4,2,128]{2,1,0:T(2,128)(2,1)} %reshape.387), calls=%async_computation.1 | async-start | bytes 4096 | tf_op jit(solution)/shard_map/all_to_all | solution.py:91
  42.0 0.6 fusion.58
  42.7 0.6 dynamic_slice.9
  43.3 0.7 reshape.381
  44.0 0.7 reshape.383
  44.6 0.2 copy.70
  44.8 0.2 reduce_window_sum.11
  45.0 2.5 %all-to-all-done.1 = bf16[4,2,128]{2,1,0:T(2,128)(2,1)S(1)} async-done(((bf16[4,2,128]{2,1,0:T(2,128)(2,1)}), bf16[4,2,128]{2,1,0:T(2,128)(2,1)S(1)}, u32[]{:S(2)}, u32[]{:S(2)}) %all-to-all-start.1) | async-done | bytes 2080 | tf_op jit(solution)/shard_map/all_to_all | solution.py:91
  47.5 3.2 %all-to-all-start.2 = ((bf16[4,2,256]{2,1,0:T(2,128)(2,1)}), bf16[4,2,256]{2,1,0:T(2,128)(2,1)S(1)}, u32[]{:S(2)}, u32[]{:S(2)}) async-start(bf16[4,2,256]{2,1,0:T(2,128)(2,1)} %reshape.383), calls=%async_computation.2 | async-start | bytes 8192 | tf_op jit(solution)/shard_map/all_to_all | solution.py:90
  50.8 0.8 multiply_reduce_fusion.3
  51.6 0.1 fusion.49
  51.7 0.1 broadcast_in_dim.10
  51.8 0.1 broadcast_in_dim.11
  51.9 0.2 fusion.45
  52.1 0.1 copy.50
  52.2 3.4 %fusion.43 = f32[8,1,8,32]{3,1,2,0:T(1,128)S(1)} fusion(f32[8,8,32,128]{3,2,1,0:T(8,128)} %bitcast.136, bf16[8,128,1,1]{1,0,2,3:T(8,128)(2,1)S(1)} %get-tuple-element.15), kind=kOutput, calls=%fused_computation.72 | convolution fusion | flops 3145728 | bytes 1058816 | tf_op jit(solution)/shard_map/sgn,sgrpn->sgrp/dot_general | solution.py:123
  55.5 1.8 %fusion.57 = (f32[64]{0:T(128)S(1)}, f32[64]{0:T(128)S(1)}, f32[64]{0:T(128)S(1)}) fusion(f32[64]{0:T(128)} %get-tuple-element.11, f32[64]{0:T(128)} %param.35, f32[64]{0:T(128)S(1)} %broadcast_in_dim.11, f32[64]{0:T(128)} %param.34, bf16[2048,64]{0,1:T(8,128)(2,1)} %param.33, bf16[2048,4]{0,1:T(4,128)(2,1)S(1)} %get-tuple-element.14, s32[]{:T(128)S(6)} %select_n.13, ...), kind=kOutput, calls=%fused_computation.90 | convolution fusion | flops 263040 | bytes 272392 | tf_op jit(solution)/shard_map/ds,dh->sh/dot_general | solution.py:86
  57.3 0.8 fusion.19
  58.1 0.1 copy.74
  58.2 0.0 all-to-all-done.2
  58.2 5.1 %all-to-all-start.3 = ((bf16[4,2,256]{2,1,0:T(2,128)(2,1)}), bf16[4,2,256]{2,1,0:T(2,128)(2,1)S(1)}, u32[]{:S(2)}, u32[]{:S(2)}) async-start(bf16[4,2,256]{2,1,0:T(2,128)(2,1)} %reshape.381), calls=%async_computation.3 | async-start | bytes 8192 | tf_op jit(solution)/shard_map/all_to_all | solution.py:89
  63.2 1.4 multiply_reduce_fusion
  64.6 0.1 copy.51
  64.7 0.1 copy.67
  64.8 0.1 reshape.384
  64.9 0.1 copy.54
  65.0 3.9 %all-to-all-done.3 = bf16[4,2,256]{2,1,0:T(2,128)(2,1)S(1)} async-done(((bf16[4,2,256]{2,1,0:T(2,128)(2,1)}), bf16[4,2,256]{2,1,0:T(2,128)(2,1)S(1)}, u32[]{:S(2)}, u32[]{:S(2)}) %all-to-all-start.3) | async-done | bytes 4128 | tf_op jit(solution)/shard_map/all_to_all | solution.py:89
  68.8 0.1 reshape.382
  68.9 0.1 copy.57
  69.0 1.3 multiply_reduce_fusion.2
  70.3 0.8 dynamic_update_slice.3
  71.1 13.6 %psum.21 = f32[4]{0:T(128)S(1)} all-reduce(f32[4]{0:T(128)S(1)} %dynamic_update_slice.3), channel_id=1, replica_groups=mesh['dp'=4,'kv'=4,'tp'=2] {'kv','tp'}, use_global_device_ids=true, to_apply=%region_8.9 | all-reduce | flops 4 | bytes 32 | tf_op jit(solution)/shard_map/psum | solution.py:141
  84.7 0.1 copy.58
  84.8 0.7 reduce.14
  85.6 0.7 reshape.389
  86.3 3.2 %all-to-all-start.4 = ((bf16[4,2,256]{2,1,0:T(2,128)(2,1)}), bf16[4,2,256]{2,1,0:T(2,128)(2,1)S(1)}, u32[]{:S(2)}, u32[]{:S(2)}) async-start(bf16[4,2,256]{2,1,0:T(2,128)(2,1)} %reshape.389), calls=%async_computation.4 | async-start | bytes 8192 | tf_op jit(solution)/shard_map/all_to_all | solution.py:143
  89.5 0.0 reduce-scatter.4.cloned.1.call-start
  89.6 5.5 %all-to-all-done.4 = bf16[4,2,256]{2,1,0:T(2,128)(2,1)S(1)} async-done(((bf16[4,2,256]{2,1,0:T(2,128)(2,1)}), bf16[4,2,256]{2,1,0:T(2,128)(2,1)S(1)}, u32[]{:S(2)}, u32[]{:S(2)}) %all-to-all-start.4) | async-done | bytes 4128 | tf_op jit(solution)/shard_map/all_to_all | solution.py:143
  95.1 0.1 reshape.390
  95.2 2.0 %convolution_bitcast_fusion.1 = f32[2048,4]{0,1:T(4,128)S(1)} fusion(bf16[16,32,2048]{2,1,0:T(8,128)(2,1)} %param.49, bf16[4,16,32]{2,1,0:T(8,128)(2,1)S(1)} %bitcast.141), kind=kOutput, calls=%fused_computation.1 | convolution fusion | flops 8388608 | bytes 2134016 | tf_op jit(solution)/shard_map/hpd,shp->ds/dot_general | solution.py:146
  97.2 3.4 %psum.22 = f32[2048,4]{0,1:T(4,128)S(1)} all-reduce(f32[2048,4]{0,1:T(4,128)S(1)} %convolution_bitcast_fusion.1), channel_id=1, replica_groups=mesh['dp'=4,'kv'=4,'tp'=2] {'tp'}, use_global_device_ids=true, to_apply=%region_9.10 | all-reduce | flops 8192 | bytes 65536 | tf_op jit(solution)/shard_map/psum | solution.py:15
  100.6 16.2 %psum.23 = f32[2048,4]{0,1:T(4,128)S(1)} all-reduce(f32[2048,4]{0,1:T(4,128)S(1)} %psum.22), channel_id=1, replica_groups=mesh['dp'=4,'kv'=4,'tp'=2] {'kv'}, use_global_device_ids=true, to_apply=%region_10.11 | all-reduce | flops 8192 | bytes 65536 | tf_op jit(solution)/shard_map/psum | solution.py:16
  116.8 0.2 fusion.13
  117.1 2.7 %convolution_multiply_fusion.3 = f32[4,704]{1,0:T(4,128)S(1)} fusion(bf16[2048,704]{0,1:T(8,128)(2,1)} %param.51, bf16[2048,4]{0,1:T(4,128)(2,1)S(1)} %get-tuple-element.6, f32[2048]{0:T(1024)S(1)} %copy-done.4, f32[4]{0:T(128)S(1)} %add_rsqrt_fusion), kind=kOutput, calls=%fused_computation.8 | convolution fusion | flops 11561728 | bytes 2919440 | tf_op jit(solution)/shard_map/ds,df->sf/dot_general | solution.py:153
  119.7 3.5 %convolution_bitcast_fusion = f32[2048,4]{0,1:T(4,128)S(1)} fusion(bf16[704,2048]{1,0:T(8,128)(2,1)S(1)} %copy-done, bf16[2048,704]{0,1:T(8,128)(2,1)} %param.52, f32[4,704]{1,0:T(4,128)S(1)} %convolution_multiply_fusion.3, bf16[2048,4]{0,1:T(4,128)(2,1)S(1)} %get-tuple-element.6, f32[2048]{0:T(1024)S(1)} %copy-done.4, f32[4]{0:T(128)S(1)} %add_rsqrt_fusion), kind=kOutput, calls=%fused_computation | convolution fusion | flops 23112960 | bytes 5835792 | tf_op jit(solution)/shard_map/fd,sf->ds/dot_general | solution.py:163
  123.2 1.4 copy.71
  124.6 0.0 reduce-scatter.4.cloned.1.call-update
  124.6 31.8 %reduce-scatter.4.cloned.1.call-done = f32[256,4]{1,0:T(8,128)} async-done(((f32[2048,4]{1,0:T(8,128)}), f32[256,4]{1,0:T(8,128)}) %reduce-scatter.4.cloned.1.call-update) | async-done | bytes 4112
  156.4 1.0 copy.72
  157.4 0.6 add_convert_fusion
  (33 shorter events, 0.2 us)
Async XLA Ops:
  6.5 113.2 %copy-start = (bf16[704,2048]{1,0:T(8,128)(2,1)S(1)}, bf16[704,2048]{1,0:T(8,128)(2,1)}, u32[]{:S(2)}) copy-start(bf16[704,2048]{1,0:T(8,128)(2,1)} %param.53) | copy-start | bytes 8650756
  23.5 13.3 %copy-start.5 = (f32[1,128,64]{1,2,0:T(8,128)S(1)}, f32[1,128,64]{1,2,0:T(8,128)}, u32[]{:S(2)}) copy-start(f32[1,128,64]{1,2,0:T(8,128)} %param.46) | copy-start | bytes 98308
  23.5 21.1 %copy-start.2 = (bf16[1,128,1024]{2,1,0:T(8,128)(2,1)S(1)}, bf16[1,128,1024]{2,1,0:T(8,128)(2,1)}, u32[]{:S(2)}) copy-start(bf16[1,128,1024]{2,1,0:T(8,128)(2,1)} %param.45) | copy-start | bytes 786436
  25.4 11.5 %all-to-all-start = ((bf16[4,2,128]{2,1,0:T(2,128)(2,1)}), bf16[4,2,128]{2,1,0:T(2,128)(2,1)S(1)}, u32[]{:S(2)}, u32[]{:S(2)}) async-start(bf16[4,2,128]{2,1,0:T(2,128)(2,1)} %reshape.385), calls=%async_computation | async-start | bytes 4096 | tf_op jit(solution)/shard_map/all_to_all | solution.py:92
  28.7 5.3 %copy-start.1 = (bf16[2048,16,32]{0,2,1:T(8,128)(2,1)S(1)}, bf16[2048,16,32]{0,2,1:T(8,128)(2,1)}, u32[]{:S(2)}) copy-start(bf16[2048,16,32]{0,2,1:T(8,128)(2,1)} %param.30) | copy-start | bytes 6291460
  34.1 34.9 %copy-start.6 = (bf16[1,3,64,32]{2,3,1,0:T(8,128)(2,1)S(1)}, bf16[1,3,64,32]{2,3,1,0:T(8,128)(2,1)}, u32[]{:S(2)}) copy-start(bf16[1,3,64,32]{2,3,1,0:T(8,128)(2,1)} %param.40) | copy-start | bytes 36868
  34.1 50.6 %copy-start.7 = (f32[64,32]{0,1:T(8,128)S(1)}, f32[64,32]{0,1:T(8,128)}, u32[]{:S(2)}) copy-start(f32[64,32]{0,1:T(8,128)} %param.48) | copy-start | bytes 24580
  35.6 8.4 %copy-start.8 = (f32[128]{0:T(128)}, f32[128]{0:T(128)S(1)}, u32[]{:S(2)}) copy-start(f32[128]{0:T(128)S(1)} %compare_convert_fusion) | copy-start | bytes 1540
  36.9 10.6 %all-to-all-start.1 = ((bf16[4,2,128]{2,1,0:T(2,128)(2,1)}), bf16[4,2,128]{2,1,0:T(2,128)(2,1)S(1)}, u32[]{:S(2)}, u32[]{:S(2)}) async-start(bf16[4,2,128]{2,1,0:T(2,128)(2,1)} %reshape.387), calls=%async_computation.1 | async-start | bytes 4096 | tf_op jit(solution)/shard_map/all_to_all | solution.py:91
  44.8 24.2 %copy-start.3 = (f32[4,64,32]{1,2,0:T(8,128)S(1)}, f32[4,64,32]{1,2,0:T(8,128)}, u32[]{:S(2)}) copy-start(f32[4,64,32]{1,2,0:T(8,128)} %param.37) | copy-start | bytes 98308
  47.5 10.6 %all-to-all-start.2 = ((bf16[4,2,256]{2,1,0:T(2,128)(2,1)}), bf16[4,2,256]{2,1,0:T(2,128)(2,1)S(1)}, u32[]{:S(2)}, u32[]{:S(2)}) async-start(bf16[4,2,256]{2,1,0:T(2,128)(2,1)} %reshape.383), calls=%async_computation.2 | async-start | bytes 8192 | tf_op jit(solution)/shard_map/all_to_all | solution.py:90
  51.8 65.3 %copy-start.4 = (f32[2048]{0:T(1024)S(1)}, f32[2048]{0:T(1024)}, u32[]{:S(2)}) copy-start(f32[2048]{0:T(1024)} %param.50) | copy-start | bytes 24580
  58.2 10.6 %all-to-all-start.3 = ((bf16[4,2,256]{2,1,0:T(2,128)(2,1)}), bf16[4,2,256]{2,1,0:T(2,128)(2,1)S(1)}, u32[]{:S(2)}, u32[]{:S(2)}) async-start(bf16[4,2,256]{2,1,0:T(2,128)(2,1)} %reshape.381), calls=%async_computation.3 | async-start | bytes 8192 | tf_op jit(solution)/shard_map/all_to_all | solution.py:89
  86.3 8.8 %all-to-all-start.4 = ((bf16[4,2,256]{2,1,0:T(2,128)(2,1)}), bf16[4,2,256]{2,1,0:T(2,128)(2,1)S(1)}, u32[]{:S(2)}, u32[]{:S(2)}) async-start(bf16[4,2,256]{2,1,0:T(2,128)(2,1)} %reshape.389), calls=%async_computation.4 | async-start | bytes 8192 | tf_op jit(solution)/shard_map/all_to_all | solution.py:143
  89.5 66.9 %reduce-scatter.4.cloned.1.call-start = ((), (), s32[]{:S(2)}) async-start(), calls=%async_computation.6 | async-start | bytes 1179648
Sparse Core Ops, SparseCore 0:
  124.7 31.6 reduce-scatter.3
